TPU v7x, 32 devices: a whole 2x2x4 slice. The times are simulated.
32 devices in a mesh: grp: 2 (over x), ep: 16 (over z, y, core).
Axes of the slice: x: 2, y: 2, z: 4, core: 2. Of those that a mesh axis runs over, the one named last changes fastest.
Arguments:
- tokens: bfloat16 [256, 2048], P(('grp', 'ep')), parts along dimension 0, may hold values from -24 to 24
- norm_gain: bfloat16 [2048], replicated, may hold values from 0.099609375 to 1.8984375
- w_query: bfloat16 [2048, 512], P('ep'), may hold values from -0.1875 to 0.1875
- w_key: bfloat16 [2048, 128], replicated, may hold values from -0.125 to 0.125
- w_value: bfloat16 [2048, 128], replicated, may hold values from -0.125 to 0.125
- w_out: bfloat16 [512, 2048], P(None, 'ep'), may hold values from -1 to 1
- cache_k: bfloat16 [256, 1024, 128], P(('grp', 'ep')), parts along dimension 0, may hold values from -6 to 6
- cache_v: bfloat16 [256, 1024, 128], P(('grp', 'ep')), parts along dimension 0, may hold values from -6 to 6
- head_offset: float32 [8], replicated, may hold values from -12 to -3
- key_shift: float32 [256, 2, 1024], P(('grp', 'ep')), parts along dimension 0, may hold values from -3 to 9
- lengths: int32 [256], P(('grp', 'ep')), parts along dimension 0, may hold values from 1 to 1024, 65536 in all
- moe_gain: bfloat16 [2048], replicated, may hold values from 0.099609375 to 1.8984375
- route_ids: int32 [256, 6], P(('grp', 'ep')), parts along dimension 0, may hold values from 0 to 15, all different within a row; in each aligned block of 8 rows (0 to 7, 8 to 15, ...) at most 6 rows name the same one
- route_score: float32 [256, 6], P(('grp', 'ep')), parts along dimension 0, may hold values from 0.05 to 1
- w_gate: bfloat16 [16, 2048, 256], P('ep'), may hold values from -0.125 to 0.125
- w_up: bfloat16 [16, 2048, 256], P('ep'), may hold values from -0.125 to 0.125
- w_down: bfloat16 [16, 256, 2048], P('ep'), may hold values from -0.375 to 0.375
- shared_gate: bfloat16 [2048, 256], replicated, may hold values from -0.125 to 0.125
- shared_up: bfloat16 [2048, 256], replicated, may hold values from -0.125 to 0.125
- shared_down: bfloat16 [256, 2048], replicated, may hold values from -0.375 to 0.375
Outputs:
- out: bfloat16 [256, 2048], P(('grp', 'ep')), parts along dimension 0
- new_key: bfloat16 [256, 128], P(('grp', 'ep')), parts along dimension 0
- new_value: bfloat16 [256, 128], P(('grp', 'ep')), parts along dimension 0
There are 2 independent parts, one for each index of `grp`. A program takes and returns all parts, laid end to end along the dimension named above; an argument that names none is the same for every part. Nothing has to cross between parts.
Inputs may be any that keep to these rules, and one draw needn't show every extreme that they name: Each sequence's cache holds lengths[b] past positions at the start; the new token stands at position lengths[b]. Some sequence of every part has exactly 1024. `route_ids`: the 6 experts of a token differ. Among the tokens of one device, no expert is named more than 6 times, a bound that some block reaches in every draw.
All inputs are finite; a program needn't handle non-finite values. No bound on the sum of `lengths` on one device may be relied on, other than what follows from the above.
Results may differ from a plain program's by a relative error of at most 0.0069.
Values may be sent and summed in bfloat16 or wider, within the bound.
A program may use at most 64 MiB of HBM per device.

v0:
```python
import math
import jax
import jax.numpy as jnp
from jax import lax
from jax.sharding import PartitionSpec as P

EPSILON = 1e-06
ROUTED_SCALE = 2.5


def norm_rows(values, gain_vec):
    mean_sq = jnp.mean(values * values, axis=-1, keepdims=True)
    return values * lax.rsqrt(mean_sq + EPSILON) * gain_vec.astype(jnp.float32)


def swiglu(row_block, gate_w, up_w, down_w):
    gate_part = jnp.dot(row_block, gate_w, preferred_element_type=jnp.float32)
    up_part = jnp.dot(row_block, up_w, preferred_element_type=jnp.float32)
    hidden = (jax.nn.silu(gate_part) * up_part).astype(jnp.bfloat16)
    return jnp.dot(hidden, down_w, preferred_element_type=jnp.float32)


def stick_weights(logits, offset, shifts, lengths):
    logits = logits + offset[None, :, :, None] + shifts[:, :, None, :]
    place_destinations = jnp.arange(logits.shape[-1], dtype=jnp.int32)
    is_live = place_destinations[None, None, None, :] < lengths[:, None, None, None]
    log_fall = jnp.where(is_live, jax.nn.log_sigmoid(-logits), 0.0)
    later_sum = lax.cumsum(log_fall, axis=3, reverse=True) - log_fall
    return jnp.where(is_live, jnp.exp(jax.nn.log_sigmoid(logits) + later_sum), 0.0).astype(
        jnp.bfloat16
    )


def attend(queries, cache_k, cache_v, offset, shifts, lengths):
    seq_count, cache_len, kv_width = cache_k.shape
    groups = shifts.shape[1]
    head_dim = kv_width // groups
    per_group = queries.shape[1] // kv_width
    query_heads = queries.reshape(seq_count, groups, per_group, head_dim)
    key_heads = cache_k.reshape(seq_count, cache_len, groups, head_dim)
    value_heads = cache_v.reshape(seq_count, cache_len, groups, head_dim)
    logits = jnp.einsum(
        "sgrd,slgd->sgrl", query_heads, key_heads, preferred_element_type=jnp.float32
    ) / math.sqrt(head_dim)
    weights = stick_weights(logits, offset.reshape(groups, per_group), shifts, lengths)
    mixed_out = jnp.einsum(
        "sgrl,slgd->sgrd", weights, value_heads, preferred_element_type=jnp.float32
    )
    return mixed_out.reshape(seq_count, queries.shape[1]).astype(jnp.bfloat16)


def shards(
    tokens,
    norm_gain,
    w_query,
    w_key,
    w_value,
    w_out,
    cache_k,
    cache_v,
    head_offset,
    key_shift,
    lengths,
    moe_gain,
    route_ids,
    route_score,
    w_gate,
    w_up,
    w_down,
    shared_gate,
    shared_up,
    shared_down,
):
    seq_dev, model_width = tokens.shape
    devices = lax.axis_size("ep")
    normed = norm_rows(tokens.astype(jnp.float32), norm_gain).astype(jnp.bfloat16)
    new_key = jnp.dot(normed, w_key, preferred_element_type=jnp.float32).astype(jnp.bfloat16)
    new_value = jnp.dot(normed, w_value, preferred_element_type=jnp.float32).astype(jnp.bfloat16)
    queries = jnp.dot(
        normed,
        lax.all_gather(w_query, "ep", axis=0, tiled=True),
        preferred_element_type=jnp.float32,
    )
    queries = queries.astype(jnp.bfloat16)
    attended = attend(queries, cache_k, cache_v, head_offset, key_shift, lengths)
    out_columns = jnp.dot(
        lax.all_gather(attended, "ep", axis=0, tiled=True),
        w_out,
        preferred_element_type=jnp.float32,
    ).astype(jnp.bfloat16)
    branch = lax.all_to_all(out_columns, "ep", split_axis=0, concat_axis=1, tiled=True)
    residual = tokens.astype(jnp.float32) + branch.astype(jnp.float32)
    moe_in = norm_rows(residual, moe_gain).astype(jnp.bfloat16)
    route_share = ROUTED_SCALE * route_score / jnp.sum(route_score, axis=1, keepdims=True)
    shared = swiglu(moe_in, shared_gate, shared_up, shared_down)
    local_count = w_gate.shape[0]
    experts_all = local_count * devices
    expert_iota = jnp.arange(experts_all, dtype=jnp.int32)
    top_count = route_ids.shape[1]
    capacity = max(2, 2 * seq_dev * top_count // experts_all)
    flat_ids = route_ids.reshape(-1)
    hit_table = (flat_ids[:, None] == expert_iota[None, :]).astype(jnp.int32)
    before = jnp.cumsum(hit_table, axis=0) - hit_table
    slot_index = jnp.sum(before * hit_table, axis=1)
    slot_place = flat_ids * capacity + slot_index
    slot_iota = jnp.arange(experts_all * capacity, dtype=jnp.int32)
    dispatch = jnp.sum(
        (slot_iota[:, None, None] == slot_place.reshape(seq_dev, top_count)[None, :, :]).astype(
            jnp.int32
        ),
        axis=2,
    ).astype(jnp.bfloat16)
    outgoing = jnp.dot(dispatch, moe_in, preferred_element_type=jnp.float32).astype(jnp.bfloat16)
    outgoing = outgoing.reshape(experts_all, capacity, model_width)
    arrived = lax.all_to_all(outgoing, "ep", split_axis=0, concat_axis=0, tiled=True)
    slot_count = arrived.shape[1]
    grouped = arrived.reshape(devices, local_count, slot_count, model_width)
    gate_part = jnp.einsum("sekd,edf->sekf", grouped, w_gate, preferred_element_type=jnp.float32)
    up_part = jnp.einsum("sekd,edf->sekf", grouped, w_up, preferred_element_type=jnp.float32)
    hidden = (jax.nn.silu(gate_part) * up_part).astype(jnp.bfloat16)
    result = jnp.einsum("sekf,efd->sekd", hidden, w_down, preferred_element_type=jnp.float32)
    result = result.astype(jnp.bfloat16).reshape(devices * local_count, slot_count, model_width)
    returned = lax.all_to_all(result, "ep", split_axis=0, concat_axis=0, tiled=True)
    returned_rows = returned.reshape(experts_all * capacity, model_width)
    picked = jnp.take(returned_rows, slot_place, axis=0).reshape(seq_dev, top_count, model_width)
    routed = jnp.sum(picked.astype(jnp.float32) * route_share[:, :, None], axis=1)
    out = (residual + routed + shared).astype(jnp.bfloat16)
    return (out, new_key, new_value)


def solution(mesh):
    placed = (
        P(("grp", "ep"), None),
        P(),
        P("ep", None),
        P(),
        P(),
        P(None, "ep"),
        P(("grp", "ep"), None, None),
        P(("grp", "ep"), None, None),
        P(),
        P(("grp", "ep"), None, None),
        P(("grp", "ep")),
        P(),
        P(("grp", "ep"), None),
        P(("grp", "ep"), None),
        P("ep", None, None),
        P("ep", None, None),
        P("ep", None, None),
        P(),
        P(),
        P(),
    )
    return jax.shard_map(
        shards,
        mesh=mesh,
        in_specs=placed,
        out_specs=(P(("grp", "ep"), None), P(("grp", "ep"), None), P(("grp", "ep"), None)),
        check_vma=False,
    )
```

profile of v0, /device:TPU:0, one launch (start us, length us, event | category | flops | bytes accessed | tf_op | source)
XLA Modules:
  0.0 228.9 jit_solution(18109210225156370043)
XLA Ops:
  7.2 0.7 all-gather.2.cloned.1.call-update
  7.9 0.7 convert_element_type.77
  8.6 4.1 %copy.39 = bf16[8,1024,128]{1,2,0:T(8,128)(2,1)} copy(bf16[8,1024,128]{2,1,0:T(8,128)(2,1)} %param.26) | data formatting | bytes 4194304 | tf_op args[6]
  12.7 0.1 add.102
  12.8 2.6 %copy.42 = bf16[8,1024,128]{1,2,0:T(8,128)(2,1)} copy(bf16[8,1024,128]{2,1,0:T(8,128)(2,1)S(1)} %copy-done.2) | data formatting | bytes 4194304 | tf_op args[7]
  15.4 0.1 reshape.160
  15.6 0.1 reduce_window_sum.27
  15.6 0.2 select_reduce_fusion
  15.8 0.1 reduce_sum.60
  15.9 0.1 copy.43
  16.0 0.1 fusion.31
  16.2 0.1 iota_compare_fusion
  16.2 38.1 %all-gather.2.cloned.1.call-done = bf16[2048,512]{1,0:T(8,128)(2,1)} async-done(((bf16[128,512]{1,0:T(8,128)(2,1)}), bf16[2048,512]{1,0:T(8,128)(2,1)}) %all-gather.2.cloned.1.call-update) | async-done | bytes 2097168 | tf_op jit(solution)/shard_map/all_gather | solution.py:81
  54.4 2.0 convolution_convert_fusion.4
  56.4 0.1 reshape.155
  56.5 3.0 %fusion.22 = (f32[8,2,4,1024]{3,2,1,0:T(4,128)S(1)}, f32[8,2,4,1024]{3,2,1,0:T(4,128)}) fusion(pred[8,1024]{1,0:T(8,128)(4,1)S(1)} %iota_compare_fusion, f32[8,2,1024]{2,1,0:T(2,128)} %param.29, f32[2,4]{1,0:T(2,128)S(1)} %add.102, bf16[8,2,4,64]{3,2,1,0:T(4,128)(2,1)S(1)} %reshape.155, bf16[8,1024,2,64]{1,3,2,0:T(8,128)(2,1)} %bitcast.79), kind=kOutput, calls=%fused_computation.35 | convolution fusion | flops 9109504 | bytes 2703392 | tf_op jit(solution)/shard_map/sgrd,slgd->sgrl/dot_general | solution.py:42
  59.5 0.8 reshape.157
  60.3 79.8 %reduce-window.6 = f32[8,2,4,8,128]{4,3,2,1,0:T(8,128)S(1)} reduce-window(f32[8,2,4,8,128]{4,3,2,1,0:T(8,128)} %reshape.157, f32[]{:T(128)} %constant.36.clone.1), window={size=1x1x1x1x128 pad=0_0x0_0x0_0x0_0x0_127}, to_apply=%region_1.2 | reduce-window | flops 8323072 | bytes 524292 | tf_op jit(solution)/shard_map/reduce-window
  140.1 0.4 copy.40
  140.6 1.3 reduce-window.9
  141.9 0.9 broadcast_add_fusion
  142.8 1.0 reduce_window_sum.26
  143.8 1.9 convolution_convert_fusion.3
  145.7 0.1 convert_element_type.82
  145.8 19.5 %all_gather.7 = bf16[128,512]{1,0:T(8,128)(2,1)S(1)} all-gather(bf16[8,512]{1,0:T(8,128)(2,1)S(1)} %convert_element_type.82), channel_id=1, replica_groups=mesh['grp'=2,'ep'=16] {'ep'}, dimensions={0}, use_global_device_ids=true | all-gather | bytes 139264 | tf_op jit(solution)/shard_map/all_gather | solution.py:87
  165.3 1.7 fusion.6
  167.0 3.6 %all-to-all-start = ((bf16[16,8,128]{2,1,0:T(8,128)(2,1)}), bf16[16,8,128]{2,1,0:T(8,128)(2,1)S(1)}, u32[]{:S(2)}, u32[]{:S(2)}) async-start(bf16[16,8,128]{2,1,0:T(8,128)(2,1)} %fusion.6), calls=%async_computation | async-start | bytes 65536 | tf_op jit(solution)/shard_map/all_to_all | solution.py:91
  170.6 0.1 convert_reduce_fusion
  170.7 6.5 %all-to-all-done = bf16[16,8,128]{2,1,0:T(8,128)(2,1)S(1)} async-done(((bf16[16,8,128]{2,1,0:T(8,128)(2,1)}), bf16[16,8,128]{2,1,0:T(8,128)(2,1)S(1)}, u32[]{:S(2)}, u32[]{:S(2)}) %all-to-all-start) | async-done | bytes 32800 | tf_op jit(solution)/shard_map/all_to_all | solution.py:91
  177.2 0.1 multiply_reduce_fusion.1
  177.3 0.3 convolution_convert_fusion.1
  177.7 0.9 reshape.161
  178.6 3.6 %all-to-all-start.1 = ((bf16[16,6,2048]{2,1,0:T(8,128)(2,1)}), bf16[16,6,2048]{2,1,0:T(8,128)(2,1)S(1)}, u32[]{:S(2)}, u32[]{:S(2)}) async-start(bf16[16,6,2048]{2,1,0:T(8,128)(2,1)} %reshape.161), calls=%async_computation.1 | async-start | bytes 1048576 | tf_op jit(solution)/shard_map/all_to_all | solution.py:115
  182.2 0.1 mul.105
  182.3 0.1 reduce_sum.64
  182.5 13.9 %all-to-all-done.1 = bf16[16,6,2048]{2,1,0:T(8,128)(2,1)S(1)} async-done(((bf16[16,6,2048]{2,1,0:T(8,128)(2,1)}), bf16[16,6,2048]{2,1,0:T(8,128)(2,1)S(1)}, u32[]{:S(2)}, u32[]{:S(2)}) %all-to-all-start.1) | async-done | bytes 393248 | tf_op jit(solution)/shard_map/all_to_all | solution.py:115
  196.4 1.6 convolution_bitcast_fusion.1
  198.1 0.8 convolution_convert_fusion
  198.9 1.0 copy.46
  199.9 4.1 %all-to-all-start.2 = ((bf16[16,6,2048]{2,1,0:T(8,128)(2,1)}), bf16[16,6,2048]{2,1,0:T(8,128)(2,1)S(1)}, u32[]{:S(2)}, u32[]{:S(2)}) async-start(bf16[16,6,2048]{2,1,0:T(8,128)(2,1)} %copy.46), calls=%async_computation.2 | async-start | bytes 1048576 | tf_op jit(solution)/shard_map/all_to_all | solution.py:123
  204.0 1.9 convolution_convert_fusion.5
  205.8 0.8 convolution_convert_fusion.6
  206.7 1.6 fusion.51
  208.2 10.0 %all-to-all-done.2 = bf16[16,6,2048]{2,1,0:T(8,128)(2,1)S(1)} async-done(((bf16[16,6,2048]{2,1,0:T(8,128)(2,1)}), bf16[16,6,2048]{2,1,0:T(8,128)(2,1)S(1)}, u32[]{:S(2)}, u32[]{:S(2)}) %all-to-all-start.2) | async-done | bytes 393248 | tf_op jit(solution)/shard_map/all_to_all | solution.py:123
  218.2 0.1 reshape.166
  218.4 0.7 gather_fusion
  219.1 0.3 multiply_reduce_fusion
  219.4 2.6 %fusion = bf16[8,2048]{1,0:T(8,128)(2,1)} fusion(bf16[256,2048]{1,0:T(8,128)(2,1)S(1)} %copy-done.5, bf16[2048,256]{1,0:T(8,128)(2,1)} %param.38, f32[8,2048]{1,0:T(8,128)S(1)} %multiply_reduce_fusion, bf16[16,8,128]{2,1,0:T(8,128)(2,1)S(1)} %all-to-all-done, bf16[8,2048]{1,0:T(8,128)(2,1)S(1)} %copy-done.1, f32[8,256]{1,0:T(8,128)S(1)} %fusion.51, ...), kind=kOutput, calls=%fused_computation.4 | convolution fusion | flops 16986112 | bytes 2277408 | tf_op jit(solution)/shard_map/dot_general | solution.py:20
  (37 shorter events, 0.5 us)
Async XLA Ops:
  7.2 190.9 %copy-start = (bf16[1,256,2048]{2,1,0:T(8,128)(2,1)S(1)}, bf16[1,256,2048]{2,1,0:T(8,128)(2,1)}, u32[]{:S(2)}) copy-start(bf16[1,256,2048]{2,1,0:T(8,128)(2,1)} %param.36) | copy-start | bytes 3145732
  7.2 47.2 %all-gather.2.cloned.1.call-start = ((), (), s32[]{:S(2)}) async-start(), calls=%async_computation.3 | async-start | bytes 2228224 | tf_op jit(solution)/shard_map/all_gather | solution.py:81
  8.6 4.1 %copy-start.11 = (f32[8]{0:T(128)S(1)}, f32[8]{0:T(128)}, u32[]{:S(2)}) copy-start(f32[8]{0:T(128)} %param.28) | copy-start | bytes 100
  8.6 4.2 %copy-start.2 = (bf16[8,1024,128]{2,1,0:T(8,128)(2,1)S(1)}, bf16[8,1024,128]{2,1,0:T(8,128)(2,1)}, u32[]{:S(2)}) copy-start(bf16[8,1024,128]{2,1,0:T(8,128)(2,1)} %param.27) | copy-start | bytes 6291460
  12.8 2.6 %copy-start.7 = (s32[8,6]{1,0:T(8,128)S(1)}, s32[8,6]{1,0:T(8,128)}, u32[]{:S(2)}) copy-start(s32[8,6]{1,0:T(8,128)} %param.32) | copy-start | bytes 580
  12.8 3.2 %copy-start.9 = (bf16[2048]{0:T(1024)(128)(2,1)S(1)}, bf16[2048]{0:T(1024)(128)(2,1)}, u32[]{:S(2)}) copy-start(bf16[2048]{0:T(1024)(128)(2,1)} %param.31) | copy-start | bytes 12292
  12.8 3.2 %copy-start.1 = (bf16[8,2048]{1,0:T(8,128)(2,1)S(1)}, bf16[8,2048]{1,0:T(8,128)(2,1)}, u32[]{:S(2)}) copy-start(bf16[8,2048]{1,0:T(8,128)(2,1)} %param.20) | copy-start | bytes 98308
  12.8 3.4 %copy-start.10 = (s32[8]{0:T(128)S(1)}, s32[8]{0:T(128)}, u32[]{:S(2)}) copy-start(s32[8]{0:T(128)} %param.30) | copy-start | bytes 100
  56.5 87.4 %copy-start.3 = (bf16[8,1024,128]{1,2,0:T(8,128)(2,1)S(1)}, bf16[8,1024,128]{1,2,0:T(8,128)(2,1)}, u32[]{:S(2)}) copy-start(bf16[8,1024,128]{1,2,0:T(8,128)(2,1)} %copy.42) | copy-start | bytes 6291460
  145.7 36.5 %copy-start.8 = (f32[8,6]{1,0:T(8,128)S(1)}, f32[8,6]{1,0:T(8,128)}, u32[]{:S(2)}) copy-start(f32[8,6]{1,0:T(8,128)} %param.33) | copy-start | bytes 580
  167.0 31.1 %copy-start.4 = (bf16[1,2048,256]{2,1,0:T(8,128)(2,1)S(1)}, bf16[1,2048,256]{2,1,0:T(8,128)(2,1)}, u32[]{:S(2)}) copy-start(bf16[1,2048,256]{2,1,0:T(8,128)(2,1)} %param.35) | copy-start | bytes 3145732
  167.0 10.2 %all-to-all-start = ((bf16[16,8,128]{2,1,0:T(8,128)(2,1)}), bf16[16,8,128]{2,1,0:T(8,128)(2,1)S(1)}, u32[]{:S(2)}, u32[]{:S(2)}) async-start(bf16[16,8,128]{2,1,0:T(8,128)(2,1)} %fusion.6), calls=%async_computation | async-start | bytes 65536 | tf_op jit(solution)/shard_map/all_to_all | solution.py:91
  178.6 17.8 %all-to-all-start.1 = ((bf16[16,6,2048]{2,1,0:T(8,128)(2,1)}), bf16[16,6,2048]{2,1,0:T(8,128)(2,1)S(1)}, u32[]{:S(2)}, u32[]{:S(2)}) async-start(bf16[16,6,2048]{2,1,0:T(8,128)(2,1)} %reshape.161), calls=%async_computation.1 | async-start | bytes 1048576 | tf_op jit(solution)/shard_map/all_to_all | solution.py:115
  198.8 7.0 %copy-start.6 = (bf16[2048,128]{1,0:T(8,128)(2,1)S(1)}, bf16[2048,128]{1,0:T(8,128)(2,1)}, u32[]{:S(2)}) copy-start(bf16[2048,128]{1,0:T(8,128)(2,1)} %param.23) | copy-start | bytes 1572868
  199.9 18.4 %all-to-all-start.2 = ((bf16[16,6,2048]{2,1,0:T(8,128)(2,1)}), bf16[16,6,2048]{2,1,0:T(8,128)(2,1)S(1)}, u32[]{:S(2)}, u32[]{:S(2)}) async-start(bf16[16,6,2048]{2,1,0:T(8,128)(2,1)} %copy.46), calls=%async_computation.2 | async-start | bytes 1048576 | tf_op jit(solution)/shard_map/all_to_all | solution.py:123
  206.7 12.8 %copy-start.5 = (bf16[256,2048]{1,0:T(8,128)(2,1)S(1)}, bf16[256,2048]{1,0:T(8,128)(2,1)}, u32[]{:S(2)}) copy-start(bf16[256,2048]{1,0:T(8,128)(2,1)} %param.39) | copy-start | bytes 3145732
Sparse Core Ops, SparseCore 0:
  10.1 44.1 all-gather.1
where the time goes:
time: 230 us; the launch traced here: 229 us
  other arithmetic  83.9 us (36%)
  waiting for transfers between devices  69.2 us (30%)
  blocking collectives  19.5 us (8%)
  matrix products  18.2 us (8%)
  between operations  14.2 us (6%)
  local copies, waits for them, and re-layouts  12.6 us (5%)
  starting transfers between devices  11.3 us (5%)
    another operation x2, other arithmetic  81.1 us
    all_gather x1, waiting for transfers between devices, shards(): lax.all_gather(w_query, 'ep', axis=0, tiled=True)  38.1 us
    all_gather x1, blocking collectives, shards(): lax.all_gather(attended, 'ep', axis=0, tiled=True)  19.5 us
    all_to_all x1, waiting for transfers between devices, shards(): lax.all_to_all(outgoing, 'ep', split_axis=0, concat_axis=0, tiled=True)  13.9 us
    all_to_all x1, waiting for transfers between devices, shards(): lax.all_to_all(result, 'ep', split_axis=0, concat_axis=0, tiled=True)  9.98 us
    unnamed x26, local copies, waits for them, and re-layouts  6.75 us
    all_to_all x1, waiting for transfers between devices, shards(): lax.all_to_all(out_columns, 'ep', split_axis=0, concat_axis=1, tiled=True)  6.52 us
  transfers between devices with their start and end apart: 4, of which 4 were waited for; matrix products, arithmetic and copies ran while one was open for 6% of the time, Pallas kernels for 0%

commit v1 on v0

--- a/solution.py
+++ b/solution.py
@@ -6,6 +6,28 @@
 
 EPSILON = 1e-06
 ROUTED_SCALE = 2.5
+
+
+def split_up(x, dim, size):
+    before, after = (x.shape[:dim], x.shape[dim + 1 :])
+    return jnp.moveaxis(x.reshape(*before, size, -1, *after), dim, 0)
+
+
+def laid_out(blocks, dim):
+    shape = list(blocks.shape[1:])
+    shape[dim] *= blocks.shape[0]
+    return jnp.moveaxis(blocks, 0, dim).reshape(shape)
+
+
+def exchange_in_pairs(shard, axis, split_dim, concat_dim):
+    size, here = (lax.axis_size(axis), lax.axis_index(axis))
+    parts = split_up(shard, split_dim, size)
+    gathered = [parts[here]]
+    for step in range(1, size):
+        sent = parts[here ^ step]
+        gathered.append(lax.ppermute(sent, axis, [(i, i ^ step) for i in range(size)]))
+    parts = jnp.stack(gathered)[here ^ jnp.arange(size)]
+    return laid_out(parts, concat_dim)
 
 
 def norm_rows(values, gain_vec):
@@ -120,7 +142,7 @@
     hidden = (jax.nn.silu(gate_part) * up_part).astype(jnp.bfloat16)
     result = jnp.einsum("sekf,efd->sekd", hidden, w_down, preferred_element_type=jnp.float32)
     result = result.astype(jnp.bfloat16).reshape(devices * local_count, slot_count, model_width)
-    returned = lax.all_to_all(result, "ep", split_axis=0, concat_axis=0, tiled=True)
+    returned = exchange_in_pairs(result, "ep", 0, 0)
     returned_rows = returned.reshape(experts_all * capacity, model_width)
     picked = jnp.take(returned_rows, slot_place, axis=0).reshape(seq_dev, top_count, model_width)
     routed = jnp.sum(picked.astype(jnp.float32) * route_share[:, :, None], axis=1)

time: 230 us -> 240 us (1.043)
  starting transfers between devices: 11.3 us -> 27.9 us
  waiting for transfers between devices: 69.2 us -> 58.7 us
  local copies, waits for them, and re-layouts: 12.6 us -> 15.5 us
    ppermute x0 -> x15, starting transfers between devices: none -> 20.8 us  [exchange_in_pairs(): lax.ppermute(sent, axis, [(i, i ^ step) for i in range(size)])]
    all_to_all x1 -> x0, waiting for transfers between devices: 9.98 us -> none  [shards(): lax.all_to_all(result, 'ep', split_axis=0, concat_axis=0, tiled=True)]
    all_to_all x1, waiting for transfers between devices: 13.9 us -> 8.83 us  [shards(): lax.all_to_all(outgoing, 'ep', split_axis=0, concat_axis=0, tiled=True)]
    ppermute x0 -> x15, waiting for transfers between devices: none -> 4.88 us  [exchange_in_pairs(): lax.ppermute(sent, axis, [(i, i ^ step) for i in range(size)])]
    all_to_all x1 -> x0, starting transfers between devices: 4.09 us -> none  [shards(): lax.all_to_all(result, 'ep', split_axis=0, concat_axis=0, tiled=True)]
    unnamed x26 -> x56, local copies, waits for them, and re-layouts: 6.75 us -> 7.86 us
  transfers between devices with their start and end apart: 4 -> 18, of which waited for: 4 -> 5; matrix products, arithmetic and copies ran while one was open for 6% -> 6% of each run, Pallas kernels for 0% -> 0%
where the time goes in v1:
time: 240 us; the launch traced here: 239 us
  other arithmetic  83.9 us (35%)
  waiting for transfers between devices  58.7 us (24%)
  starting transfers between devices  27.9 us (12%)
  blocking collectives  19.5 us (8%)
  matrix products  19.2 us (8%)
  local copies, waits for them, and re-layouts  15.5 us (6%)
  between operations  14.5 us (6%)
    another operation x2, other arithmetic  81.1 us
    all_gather x1, waiting for transfers between devices, shards(): lax.all_gather(w_query, 'ep', axis=0, tiled=True)  37.8 us
    ppermute x15, starting transfers between devices, exchange_in_pairs(): lax.ppermute(sent, axis, [(i, i ^ step) for i in range(size)])  20.8 us
    all_gather x1, blocking collectives, shards(): lax.all_gather(attended, 'ep', axis=0, tiled=True)  19.5 us
    all_to_all x1, waiting for transfers between devices, shards(): lax.all_to_all(outgoing, 'ep', split_axis=0, concat_axis=0, tiled=True)  8.83 us
    unnamed x56, local copies, waits for them, and re-layouts  7.86 us
    all_to_all x1, waiting for transfers between devices, shards(): lax.all_to_all(out_columns, 'ep', split_axis=0, concat_axis=1, tiled=True)  6.58 us
    ppermute x15, waiting for transfers between devices, exchange_in_pairs(): lax.ppermute(sent, axis, [(i, i ^ step) for i in range(size)])  4.88 us
  transfers between devices with their start and end apart: 18, of which 5 were waited for; matrix products, arithmetic and copies ran while one was open for 6% of the time, Pallas kernels for 0%

profile of v1, /device:TPU:0, one launch (start us, length us, event | category | flops | bytes accessed | tf_op | source)
XLA Modules:
  0.0 239.2 jit_solution(14597139561668581975)
XLA Ops:
  7.2 0.7 all-gather.2.cloned.1.call-update
  7.9 0.7 convert_element_type.77
  8.6 4.1 %copy.382 = bf16[8,1024,128]{1,2,0:T(8,128)(2,1)} copy(bf16[8,1024,128]{2,1,0:T(8,128)(2,1)} %param.26) | data formatting | bytes 4194304 | tf_op args[6]
  12.8 2.6 %copy.385 = bf16[8,1024,128]{1,2,0:T(8,128)(2,1)} copy(bf16[8,1024,128]{2,1,0:T(8,128)(2,1)S(1)} %copy-done.2) | data formatting | bytes 4194304 | tf_op args[7]
  16.6 37.8 %all-gather.2.cloned.1.call-done = bf16[2048,512]{1,0:T(8,128)(2,1)} async-done(((bf16[128,512]{1,0:T(8,128)(2,1)}), bf16[2048,512]{1,0:T(8,128)(2,1)}) %all-gather.2.cloned.1.call-update) | async-done | bytes 2097168 | tf_op jit(solution)/shard_map/all_gather | solution.py:103
  54.4 2.0 convolution_convert_fusion.4
  56.5 3.0 %fusion.22 = (f32[8,2,4,1024]{3,2,1,0:T(4,128)S(1)}, f32[8,2,4,1024]{3,2,1,0:T(4,128)}) fusion(pred[8,1024]{1,0:T(8,128)(4,1)S(1)} %iota_compare_fusion, f32[8,2,1024]{2,1,0:T(2,128)} %param.29, f32[2,4]{1,0:T(2,128)S(1)} %add.160, bf16[8,2,4,64]{3,2,1,0:T(4,128)(2,1)S(1)} %reshape.215, bf16[8,1024,2,64]{1,3,2,0:T(8,128)(2,1)} %bitcast.283), kind=kOutput, calls=%fused_computation.36 | convolution fusion | flops 9109504 | bytes 2703392 | tf_op jit(solution)/shard_map/sgrd,slgd->sgrl/dot_general | solution.py:64
  59.5 0.8 reshape.217
  60.3 79.8 %reduce-window.6 = f32[8,2,4,8,128]{4,3,2,1,0:T(8,128)S(1)} reduce-window(f32[8,2,4,8,128]{4,3,2,1,0:T(8,128)} %reshape.217, f32[]{:T(128)} %constant.27.clone.1), window={size=1x1x1x1x128 pad=0_0x0_0x0_0x0_0x0_127}, to_apply=%region_1.2 | reduce-window | flops 8323072 | bytes 524292 | tf_op jit(solution)/shard_map/reduce-window
  140.1 0.4 copy.383
  140.5 1.3 reduce-window.9
  141.9 0.8 broadcast_add_fusion
  142.7 1.0 reduce_window_sum.26
  143.8 1.9 convolution_convert_fusion.3
  145.8 19.5 %all_gather.7 = bf16[128,512]{1,0:T(8,128)(2,1)S(1)} all-gather(bf16[8,512]{1,0:T(8,128)(2,1)S(1)} %convert_element_type.82), channel_id=1, replica_groups=mesh['grp'=2,'ep'=16] {'ep'}, dimensions={0}, use_global_device_ids=true | all-gather | bytes 139264 | tf_op jit(solution)/shard_map/all_gather | solution.py:109
  165.2 1.7 fusion.6
  166.9 3.5 %all-to-all-start = ((bf16[16,8,128]{2,1,0:T(8,128)(2,1)}), bf16[16,8,128]{2,1,0:T(8,128)(2,1)S(1)}, u32[]{:S(2)}, u32[]{:S(2)}) async-start(bf16[16,8,128]{2,1,0:T(8,128)(2,1)} %fusion.6), calls=%async_computation | async-start | bytes 65536 | tf_op jit(solution)/shard_map/all_to_all | solution.py:113
  170.4 6.6 %all-to-all-done = bf16[16,8,128]{2,1,0:T(8,128)(2,1)S(1)} async-done(((bf16[16,8,128]{2,1,0:T(8,128)(2,1)}), bf16[16,8,128]{2,1,0:T(8,128)(2,1)S(1)}, u32[]{:S(2)}, u32[]{:S(2)}) %all-to-all-start) | async-done | bytes 32800 | tf_op jit(solution)/shard_map/all_to_all | solution.py:113
  177.1 0.3 convolution_convert_fusion.1
  177.5 0.9 reshape.221
  178.4 3.6 %all-to-all-start.1 = ((bf16[16,6,2048]{2,1,0:T(8,128)(2,1)}), bf16[16,6,2048]{2,1,0:T(8,128)(2,1)S(1)}, u32[]{:S(2)}, u32[]{:S(2)}) async-start(bf16[16,6,2048]{2,1,0:T(8,128)(2,1)} %reshape.221), calls=%async_computation.1 | async-start | bytes 1048576 | tf_op jit(solution)/shard_map/all_to_all | solution.py:137
  182.1 1.9 convolution_convert_fusion.5
  184.0 1.9 convolution_convert_fusion.6
  185.9 1.5 fusion.52
  187.4 8.8 %all-to-all-done.1 = bf16[16,6,2048]{2,1,0:T(8,128)(2,1)S(1)} async-done(((bf16[16,6,2048]{2,1,0:T(8,128)(2,1)}), bf16[16,6,2048]{2,1,0:T(8,128)(2,1)S(1)}, u32[]{:S(2)}, u32[]{:S(2)}) %all-to-all-start.1) | async-done | bytes 393248 | tf_op jit(solution)/shard_map/all_to_all | solution.py:137
  196.2 1.6 convolution_bitcast_fusion.1
  197.9 0.8 convolution_convert_fusion
  198.7 1.2 dynamic-slice_bitcast_fusion
  200.1 1.3 collective-permute-start.1
  201.4 0.5 collective-permute-start.2
  202.0 1.4 collective-permute-start.3
  203.5 0.5 collective-permute-start.4
  204.2 2.1 collective-permute-start.5
  206.4 0.5 collective-permute-start.6
  206.9 2.4 collective-permute-start.7
  209.3 0.3 collective-permute-start.8
  209.6 1.8 collective-permute-start.9
  211.4 1.7 collective-permute-start.10
  213.1 1.8 collective-permute-start.11
  215.0 1.7 collective-permute-start.12
  216.7 3.0 %collective-permute-start.13 = (bf16[1,6,2048]{2,1,0:T(8,128)(2,1)S(1)}, bf16[1,6,2048]{2,1,0:T(8,128)(2,1)S(1)}, u32[]{:S(2)}, u32[]{:S(2)}) collective-permute-start(bf16[1,6,2048]{2,1,0:T(8,128)(2,1)S(1)} %bitcast.287), channel_id=1, source_target_pairs={{0,14},{1,15},{2,12},{3,13},{4,10},{5,11},{6,8},{7,9},{8,6},{9,7},... | collective-permute-start | bytes 73736 | tf_op jit(solution)/shard_map/ppermute | solution.py:28
  219.7 1.5 collective-permute-start.14
  221.2 2.1 collective-permute-done.13
  223.3 2.7 %collective-permute-done.14 = bf16[1,6,2048]{2,1,0:T(8,128)(2,1)S(1)} collective-permute-done((bf16[1,6,2048]{2,1,0:T(8,128)(2,1)S(1)}, bf16[1,6,2048]{2,1,0:T(8,128)(2,1)S(1)}, u32[]{:S(2)}, u32[]{:S(2)}) %collective-permute-start.14) | collective-permute-done | bytes 24608 | tf_op jit(solution)/shard_map/ppermute | solution.py:28
  226.0 0.8 copy-done.6
  226.8 1.7 gather_fusion
  228.7 0.7 gather_fusion.1
  229.8 2.6 %fusion = bf16[8,2048]{1,0:T(8,128)(2,1)} fusion(bf16[256,2048]{1,0:T(8,128)(2,1)S(1)} %copy-done.5, bf16[2048,256]{1,0:T(8,128)(2,1)} %param.38, f32[8,2048]{1,0:T(8,128)S(1)} %multiply_reduce_fusion, bf16[16,8,128]{2,1,0:T(8,128)(2,1)S(1)} %all-to-all-done, bf16[8,2048]{1,0:T(8,128)(2,1)S(1)} %copy-done.1, f32[8,256]{1,0:T(8,128)S(1)} %fusion.52, ...), kind=kOutput, calls=%fused_computation.5 | convolution fusion | flops 16986112 | bytes 2277408 | tf_op jit(solution)/shard_map/dot_general | solution.py:42
  (99 shorter events, 2.8 us)
Async XLA Ops:
  7.2 190.7 %copy-start = (bf16[1,256,2048]{2,1,0:T(8,128)(2,1)S(1)}, bf16[1,256,2048]{2,1,0:T(8,128)(2,1)}, u32[]{:S(2)}) copy-start(bf16[1,256,2048]{2,1,0:T(8,128)(2,1)} %param.36) | copy-start | bytes 3145732
  7.2 47.2 %all-gather.2.cloned.1.call-start = ((), (), s32[]{:S(2)}) async-start(), calls=%async_computation.2 | async-start | bytes 2228224 | tf_op jit(solution)/shard_map/all_gather | solution.py:103
  8.6 4.1 %copy-start.11 = (f32[8]{0:T(128)S(1)}, f32[8]{0:T(128)}, u32[]{:S(2)}) copy-start(f32[8]{0:T(128)} %param.28) | copy-start | bytes 100
  8.6 4.1 %copy-start.2 = (bf16[8,1024,128]{2,1,0:T(8,128)(2,1)S(1)}, bf16[8,1024,128]{2,1,0:T(8,128)(2,1)}, u32[]{:S(2)}) copy-start(bf16[8,1024,128]{2,1,0:T(8,128)(2,1)} %param.27) | copy-start | bytes 6291460
  12.8 2.6 %copy-start.7 = (s32[8,6]{1,0:T(8,128)S(1)}, s32[8,6]{1,0:T(8,128)}, u32[]{:S(2)}) copy-start(s32[8,6]{1,0:T(8,128)} %param.32) | copy-start | bytes 580
  12.8 3.2 %copy-start.9 = (bf16[2048]{0:T(1024)(128)(2,1)S(1)}, bf16[2048]{0:T(1024)(128)(2,1)}, u32[]{:S(2)}) copy-start(bf16[2048]{0:T(1024)(128)(2,1)} %param.31) | copy-start | bytes 12292
  12.8 3.3 %copy-start.8 = (f32[8,6]{1,0:T(8,128)S(1)}, f32[8,6]{1,0:T(8,128)}, u32[]{:S(2)}) copy-start(f32[8,6]{1,0:T(8,128)} %param.33) | copy-start | bytes 580
  12.8 3.5 %copy-start.1 = (bf16[8,2048]{1,0:T(8,128)(2,1)S(1)}, bf16[8,2048]{1,0:T(8,128)(2,1)}, u32[]{:S(2)}) copy-start(bf16[8,2048]{1,0:T(8,128)(2,1)} %param.20) | copy-start | bytes 98308
  12.8 3.7 %copy-start.10 = (s32[8]{0:T(128)S(1)}, s32[8]{0:T(128)}, u32[]{:S(2)}) copy-start(s32[8]{0:T(128)} %param.30) | copy-start | bytes 100
  56.5 87.3 %copy-start.3 = (bf16[8,1024,128]{1,2,0:T(8,128)(2,1)S(1)}, bf16[8,1024,128]{1,2,0:T(8,128)(2,1)}, u32[]{:S(2)}) copy-start(bf16[8,1024,128]{1,2,0:T(8,128)(2,1)} %copy.385) | copy-start | bytes 6291460
  166.9 10.1 %all-to-all-start = ((bf16[16,8,128]{2,1,0:T(8,128)(2,1)}), bf16[16,8,128]{2,1,0:T(8,128)(2,1)S(1)}, u32[]{:S(2)}, u32[]{:S(2)}) async-start(bf16[16,8,128]{2,1,0:T(8,128)(2,1)} %fusion.6), calls=%async_computation | async-start | bytes 65536 | tf_op jit(solution)/shard_map/all_to_all | solution.py:113
  178.4 17.8 %all-to-all-start.1 = ((bf16[16,6,2048]{2,1,0:T(8,128)(2,1)}), bf16[16,6,2048]{2,1,0:T(8,128)(2,1)S(1)}, u32[]{:S(2)}, u32[]{:S(2)}) async-start(bf16[16,6,2048]{2,1,0:T(8,128)(2,1)} %reshape.221), calls=%async_computation.1 | async-start | bytes 1048576 | tf_op jit(solution)/shard_map/all_to_all | solution.py:137
  182.0 15.9 %copy-start.4 = (bf16[1,2048,256]{2,1,0:T(8,128)(2,1)S(1)}, bf16[1,2048,256]{2,1,0:T(8,128)(2,1)}, u32[]{:S(2)}) copy-start(bf16[1,2048,256]{2,1,0:T(8,128)(2,1)} %param.35) | copy-start | bytes 3145732
  199.9 4.3 %collective-permute-start = (bf16[1,6,2048]{2,1,0:T(8,128)(2,1)S(1)}, bf16[1,6,2048]{2,1,0:T(8,128)(2,1)S(1)}, u32[]{:S(2)}, u32[]{:S(2)}) collective-permute-start(bf16[1,6,2048]{2,1,0:T(8,128)(2,1)S(1)} %bitcast.300), channel_id=1, source_target_pairs={{0,1},{1,0},{2,3},{3,2},{4,5},{5,4},{6,7},{7,6},{8,9},{9,8},{10,11... | collective-permute-start | bytes 73736 | tf_op jit(solution)/shard_map/ppermute | solution.py:28
  200.1 6.3 %collective-permute-start.1 = (bf16[1,6,2048]{2,1,0:T(8,128)(2,1)S(1)}, bf16[1,6,2048]{2,1,0:T(8,128)(2,1)S(1)}, u32[]{:S(2)}, u32[]{:S(2)}) collective-permute-start(bf16[1,6,2048]{2,1,0:T(8,128)(2,1)S(1)} %bitcast.299), channel_id=1, source_target_pairs={{0,2},{1,3},{2,0},{3,1},{4,6},{5,7},{6,4},{7,5},{8,10},{9,11},{10,... | collective-permute-start | bytes 73736 | tf_op jit(solution)/shard_map/ppermute | solution.py:28
  201.4 5.5 %collective-permute-start.2 = (bf16[1,6,2048]{2,1,0:T(8,128)(2,1)S(1)}, bf16[1,6,2048]{2,1,0:T(8,128)(2,1)S(1)}, u32[]{:S(2)}, u32[]{:S(2)}) collective-permute-start(bf16[1,6,2048]{2,1,0:T(8,128)(2,1)S(1)} %bitcast.298), channel_id=1, source_target_pairs={{0,3},{1,2},{2,1},{3,0},{4,7},{5,6},{6,5},{7,4},{8,11},{9,10},{10,... | collective-permute-start | bytes 73736 | tf_op jit(solution)/shard_map/ppermute | solution.py:28
  202.0 7.3 %collective-permute-start.3 = (bf16[1,6,2048]{2,1,0:T(8,128)(2,1)S(1)}, bf16[1,6,2048]{2,1,0:T(8,128)(2,1)S(1)}, u32[]{:S(2)}, u32[]{:S(2)}) collective-permute-start(bf16[1,6,2048]{2,1,0:T(8,128)(2,1)S(1)} %bitcast.297), channel_id=1, source_target_pairs={{0,4},{1,5},{2,6},{3,7},{4,0},{5,1},{6,2},{7,3},{8,12},{9,13},{10,... | collective-permute-start | bytes 73736 | tf_op jit(solution)/shard_map/ppermute | solution.py:28
  203.5 6.1 %collective-permute-start.4 = (bf16[1,6,2048]{2,1,0:T(8,128)(2,1)S(1)}, bf16[1,6,2048]{2,1,0:T(8,128)(2,1)S(1)}, u32[]{:S(2)}, u32[]{:S(2)}) collective-permute-start(bf16[1,6,2048]{2,1,0:T(8,128)(2,1)S(1)} %bitcast.296), channel_id=1, source_target_pairs={{0,5},{1,4},{2,7},{3,6},{4,1},{5,0},{6,3},{7,2},{8,13},{9,12},{10,... | collective-permute-start | bytes 73736 | tf_op jit(solution)/shard_map/ppermute | solution.py:28
  204.2 7.2 %collective-permute-start.5 = (bf16[1,6,2048]{2,1,0:T(8,128)(2,1)S(1)}, bf16[1,6,2048]{2,1,0:T(8,128)(2,1)S(1)}, u32[]{:S(2)}, u32[]{:S(2)}) collective-permute-start(bf16[1,6,2048]{2,1,0:T(8,128)(2,1)S(1)} %bitcast.295), channel_id=1, source_target_pairs={{0,6},{1,7},{2,4},{3,5},{4,2},{5,3},{6,0},{7,1},{8,14},{9,15},{10,... | collective-permute-start | bytes 73736 | tf_op jit(solution)/shard_map/ppermute | solution.py:28
  206.4 6.8 %collective-permute-start.6 = (bf16[1,6,2048]{2,1,0:T(8,128)(2,1)S(1)}, bf16[1,6,2048]{2,1,0:T(8,128)(2,1)S(1)}, u32[]{:S(2)}, u32[]{:S(2)}) collective-permute-start(bf16[1,6,2048]{2,1,0:T(8,128)(2,1)S(1)} %bitcast.294), channel_id=1, source_target_pairs={{0,7},{1,6},{2,5},{3,4},{4,3},{5,2},{6,1},{7,0},{8,15},{9,14},{10,... | collective-permute-start | bytes 73736 | tf_op jit(solution)/shard_map/ppermute | solution.py:28
  206.9 8.1 %collective-permute-start.7 = (bf16[1,6,2048]{2,1,0:T(8,128)(2,1)S(1)}, bf16[1,6,2048]{2,1,0:T(8,128)(2,1)S(1)}, u32[]{:S(2)}, u32[]{:S(2)}) collective-permute-start(bf16[1,6,2048]{2,1,0:T(8,128)(2,1)S(1)} %bitcast.293), channel_id=1, source_target_pairs={{0,8},{1,9},{2,10},{3,11},{4,12},{5,13},{6,14},{7,15},{8,0},{9,1},... | collective-permute-start | bytes 73736 | tf_op jit(solution)/shard_map/ppermute | solution.py:28
  209.3 7.4 %collective-permute-start.8 = (bf16[1,6,2048]{2,1,0:T(8,128)(2,1)S(1)}, bf16[1,6,2048]{2,1,0:T(8,128)(2,1)S(1)}, u32[]{:S(2)}, u32[]{:S(2)}) collective-permute-start(bf16[1,6,2048]{2,1,0:T(8,128)(2,1)S(1)} %bitcast.292), channel_id=1, source_target_pairs={{0,9},{1,8},{2,11},{3,10},{4,13},{5,12},{6,15},{7,14},{8,1},{9,0},... | collective-permute-start | bytes 73736 | tf_op jit(solution)/shard_map/ppermute | solution.py:28
  209.6 10.1 %collective-permute-start.9 = (bf16[1,6,2048]{2,1,0:T(8,128)(2,1)S(1)}, bf16[1,6,2048]{2,1,0:T(8,128)(2,1)S(1)}, u32[]{:S(2)}, u32[]{:S(2)}) collective-permute-start(bf16[1,6,2048]{2,1,0:T(8,128)(2,1)S(1)} %bitcast.291), channel_id=1, source_target_pairs={{0,10},{1,11},{2,8},{3,9},{4,14},{5,15},{6,12},{7,13},{8,2},{9,3},... | collective-permute-start | bytes 73736 | tf_op jit(solution)/shard_map/ppermute | solution.py:28
  211.4 9.7 %collective-permute-start.10 = (bf16[1,6,2048]{2,1,0:T(8,128)(2,1)S(1)}, bf16[1,6,2048]{2,1,0:T(8,128)(2,1)S(1)}, u32[]{:S(2)}, u32[]{:S(2)}) collective-permute-start(bf16[1,6,2048]{2,1,0:T(8,128)(2,1)S(1)} %bitcast.290), channel_id=1, source_target_pairs={{0,11},{1,10},{2,9},{3,8},{4,15},{5,14},{6,13},{7,12},{8,3},{9,2},... | collective-permute-start | bytes 73736 | tf_op jit(solution)/shard_map/ppermute | solution.py:28
  213.1 8.0 %collective-permute-start.11 = (bf16[1,6,2048]{2,1,0:T(8,128)(2,1)S(1)}, bf16[1,6,2048]{2,1,0:T(8,128)(2,1)S(1)}, u32[]{:S(2)}, u32[]{:S(2)}) collective-permute-start(bf16[1,6,2048]{2,1,0:T(8,128)(2,1)S(1)} %bitcast.289), channel_id=1, source_target_pairs={{0,12},{1,13},{2,14},{3,15},{4,8},{5,9},{6,10},{7,11},{8,4},{9,5},... | collective-permute-start | bytes 73736 | tf_op jit(solution)/shard_map/ppermute | solution.py:28
  215.0 6.2 %collective-permute-start.12 = (bf16[1,6,2048]{2,1,0:T(8,128)(2,1)S(1)}, bf16[1,6,2048]{2,1,0:T(8,128)(2,1)S(1)}, u32[]{:S(2)}, u32[]{:S(2)}) collective-permute-start(bf16[1,6,2048]{2,1,0:T(8,128)(2,1)S(1)} %bitcast.288), channel_id=1, source_target_pairs={{0,13},{1,12},{2,15},{3,14},{4,9},{5,8},{6,11},{7,10},{8,5},{9,4},... | collective-permute-start | bytes 73736 | tf_op jit(solution)/shard_map/ppermute | solution.py:28
  216.7 6.6 %collective-permute-start.13 = (bf16[1,6,2048]{2,1,0:T(8,128)(2,1)S(1)}, bf16[1,6,2048]{2,1,0:T(8,128)(2,1)S(1)}, u32[]{:S(2)}, u32[]{:S(2)}) collective-permute-start(bf16[1,6,2048]{2,1,0:T(8,128)(2,1)S(1)} %bitcast.287), channel_id=1, source_target_pairs={{0,14},{1,15},{2,12},{3,13},{4,10},{5,11},{6,8},{7,9},{8,6},{9,7},... | collective-permute-start | bytes 73736 | tf_op jit(solution)/shard_map/ppermute | solution.py:28
  219.7 6.4 %collective-permute-start.14 = (bf16[1,6,2048]{2,1,0:T(8,128)(2,1)S(1)}, bf16[1,6,2048]{2,1,0:T(8,128)(2,1)S(1)}, u32[]{:S(2)}, u32[]{:S(2)}) collective-permute-start(bf16[1,6,2048]{2,1,0:T(8,128)(2,1)S(1)} %bitcast.286), channel_id=1, source_target_pairs={{0,15},{1,14},{2,13},{3,12},{4,11},{5,10},{6,9},{7,8},{8,7},{9,6},... | collective-permute-start | bytes 73736 | tf_op jit(solution)/shard_map/ppermute | solution.py:28
  226.0 0.8 copy-start.6
  226.8 2.9 %copy-start.5 = (bf16[256,2048]{1,0:T(8,128)(2,1)S(1)}, bf16[256,2048]{1,0:T(8,128)(2,1)}, u32[]{:S(2)}) copy-start(bf16[256,2048]{1,0:T(8,128)(2,1)} %param.39) | copy-start | bytes 3145732
Sparse Core Ops, SparseCore 0:
  10.1 44.1 all-gather.1
